TPU v7x, 32 devices: a whole 2x2x4 slice. The times are simulated.
32 devices in a mesh: fs: 4 (over z), tp: 4 (over y, x), rep: 2 (over core).
Axes of the slice: x: 2, y: 2, z: 4, core: 2. Of those that a mesh axis runs over, the one named last changes fastest.
Arguments:
- up_weight: float32 [2048, 8192], P('fs', ('tp', 'rep')), may hold values from -0.125 to 0.125
- up_momentum: float32 [2048, 8192], P('fs', ('tp', 'rep')), may hold values from -24 to 24
- up_grads: bfloat16 [2, 2048, 8192], P('rep', 'fs', 'tp'), may hold values from -2.09375 to 2.09375
- out_weight: float32 [2048, 2048], P('fs', ('tp', 'rep')), may hold values from -0.125 to 0.125
- out_momentum: float32 [2048, 2048], P('fs', ('tp', 'rep')), may hold values from -24 to 24
- out_grads: bfloat16 [2, 2048, 2048], P('rep', 'fs', 'tp'), may hold values from -2.09375 to 2.09375
Outputs:
- up_weight_new: float32 [2048, 8192], P('fs', ('tp', 'rep'))
- up_momentum_new: float32 [2048, 8192], P('fs', ('tp', 'rep'))
- up_direction: float32 [2048, 8192], P('fs', ('tp', 'rep'))
- out_weight_new: float32 [2048, 2048], P('fs', ('tp', 'rep'))
- out_momentum_new: float32 [2048, 2048], P('fs', ('tp', 'rep'))
- out_direction: float32 [2048, 2048], P('fs', ('tp', 'rep'))
All inputs are finite; a program needn't handle non-finite values.
Results may differ from a plain program's by a relative error of at most 0.039.
Values may be sent and summed in bfloat16 or wider, within the bound.
A program may use at most 64 MiB of HBM per device.

v0:
```python
import math

import jax
import jax.numpy as jnp
from jax import lax
from jax.sharding import PartitionSpec as P

ITERS = 3
MOMENT = 0.9
RATE = 0.02
COEF_A = 3.4445
COEF_B = -4.775
COEF_C = 2.0315
BF = jnp.bfloat16
F32 = jnp.float32
ROLES = 2
CUTS = 8


def mm(a, b):
    return jnp.dot(a, b, preferred_element_type=F32)


def mm_t(a, b):
    return lax.dot_general(a, b, (((1,), (1,)), ((), ())), preferred_element_type=F32)


def reduced_grad(grads):
    size = lax.axis_size("rep")
    rows, cols = grads.shape
    pieces = grads.reshape(rows, size, cols // size).transpose(1, 0, 2)
    pieces = lax.all_to_all(pieces, "rep", split_axis=0, concat_axis=0, tiled=True)
    return jnp.sum(pieces.astype(F32), axis=0)


def to_columns(values):
    size = lax.axis_size("fs")
    rows, cols = values.shape
    pieces = values.reshape(rows, size, cols // size).transpose(1, 0, 2)
    pieces = lax.all_to_all(pieces, "fs", split_axis=0, concat_axis=0, tiled=True)
    return pieces.reshape(size * rows, cols // size)


def to_rows(values):
    size = lax.axis_size("fs")
    rows, cols = values.shape
    pieces = values.reshape(size, rows // size, cols)
    pieces = lax.all_to_all(pieces, "fs", split_axis=0, concat_axis=0, tiled=True)
    return pieces.transpose(1, 0, 2).reshape(rows // size, cols * size)


def swap_pairs(values):
    size = lax.axis_size("rep")
    return lax.ppermute(values, "rep", [(i, i ^ 1) for i in range(size)])


def pack_gram(x):
    step = x.shape[0] // CUTS
    rows = []
    for i in range(CUTS // 2):
        j = CUTS - 1 - i
        rows.append(
            jnp.concatenate(
                [
                    mm_t(x[i * step : (i + 1) * step], x[i * step :]).astype(BF),
                    mm_t(x[j * step : (j + 1) * step], x[j * step :]).astype(BF),
                ],
                axis=1,
            )
        )
    return jnp.concatenate(rows, axis=0)


def unpack_gram(packed):
    step = packed.shape[0] * 2 // CUTS
    upper = {}
    for i in range(CUTS // 2):
        row = packed[i * step : (i + 1) * step]
        upper[i] = row[:, : (CUTS - i) * step]
        upper[CUTS - 1 - i] = row[:, (CUTS - i) * step :]
    full = []
    for i in range(CUTS):
        left = [upper[j][:, (i - j) * step : (i - j + 1) * step].T for j in range(i)]
        full.append(jnp.concatenate(left + [upper[i]], axis=1))
    return jnp.concatenate(full, axis=0)


def next_gram(a):
    square = mm(a, a)
    q = (COEF_B * a.astype(F32) + COEF_C * square).astype(BF)
    w = (COEF_A * a.astype(F32) + mm(q, a)).astype(BF)
    return (COEF_A * w.astype(F32) + mm(q, w)).astype(BF)


def on_device(up_weight, up_momentum, up_grads, out_weight, out_momentum, out_grads):
    even = lax.axis_index("rep") % 2 == 0
    up_moment = MOMENT * up_momentum + reduced_grad(up_grads[0])
    out_moment = MOMENT * out_momentum + reduced_grad(out_grads[0])
    up = to_columns(up_moment.astype(BF))
    out = to_columns(out_moment.astype(BF))
    width, narrow = up.shape[1], out.shape[1]
    out = jnp.pad(out, ((0, 0), (0, width - narrow)))
    other = swap_pairs(jnp.where(even, out, up))
    values = jnp.concatenate([jnp.where(even, up, out), other], axis=1)
    gram = unpack_gram(lax.psum(pack_gram(values), ("fs", "tp"))) if lax.axis_size("rep") == 2 else None
    if gram is None:
        size = lax.axis_size("rep")
        groups = [[i for i in range(size) if i % 2 == k] for k in range(2)]
        packed = lax.psum(pack_gram(values), ("fs", "tp"))
        packed = lax.psum(packed, "rep", axis_index_groups=groups)
        gram = unpack_gram(packed)
    gram = gram.astype(F32)
    square = 1.0 / (jnp.sqrt(jnp.sum(gram * gram)) + 1.0)
    factor = jnp.sqrt(square)
    a = (gram * square).astype(BF)
    current = values.astype(F32)
    for iteration in range(ITERS):
        y = mm(a, current.astype(BF))
        if iteration == 0:
            y = factor * y
            current = factor * current
        z = mm(a, y.astype(BF))
        current = COEF_A * current + COEF_B * y + COEF_C * z
        if iteration < ITERS - 1:
            a = next_gram(a)
    final = current.astype(BF)
    mine, other = final[:, :width], swap_pairs(final[:, width:])
    up = to_rows(jnp.where(even, mine, other)).astype(F32)
    out = to_rows(jnp.where(even, other, mine)[:, :narrow]).astype(F32)
    group = lax.axis_size("tp") * lax.axis_size("rep")
    up_direction = up * math.sqrt(up_weight.shape[1] * group)
    out_direction = out * math.sqrt(out_weight.shape[1] * group)
    return (
        up_weight - RATE * up_direction,
        up_moment,
        up_direction,
        out_weight - RATE * out_direction,
        out_moment,
        out_direction,
    )


def solution(mesh):
    flat = P("fs", ("tp", "rep"))
    grads = P("rep", "fs", "tp")
    return jax.shard_map(
        on_device,
        mesh=mesh,
        in_specs=(flat, flat, grads, flat, flat, grads),
        out_specs=(flat,) * 6,
        check_vma=False,
    )
```

profile of v0, /device:TPU:0, one launch (start us, length us, event | category | flops | bytes accessed | tf_op | source)
XLA Modules:
  0.0 534.9 jit_solution(14960733986047631695)
XLA Ops:
  7.2 1.3 copy.128
  8.5 1.0 copy.129
  9.5 3.5 all-to-all-start.2
  13.0 2.9 copy.125
  15.9 2.4 copy.126
  18.2 3.8 all-to-all-start
  22.1 0.9 fusion.65
  23.0 0.8 copy.131
  23.8 1.1 all-to-all-done
  24.9 6.3 %all-to-all-start.3 = ((bf16[4,512,64]{1,2,0:T(8,128)(2,1)}), bf16[4,512,64]{1,2,0:T(8,128)(2,1)S(1)}, u32[]{:S(2)}, u32[]{:S(2)}) async-start(bf16[4,512,64]{1,2,0:T(8,128)(2,1)} %bitcast.7), calls=%async_computation.3 | async-start | bytes 524288 | tf_op jit(solution)/shard_map/all_to_all | solution.py:40
  31.7 3.4 fusion.64
  35.1 1.0 copy.202
  36.2 4.3 all-to-all-done.3
  40.4 3.5 all-to-all-start.1
  44.3 23.9 %all-to-all-done.1 = bf16[4,512,256]{2,1,0:T(8,128)(2,1)S(1)} async-done(((bf16[4,512,256]{2,1,0:T(8,128)(2,1)}), bf16[4,512,256]{2,1,0:T(8,128)(2,1)S(1)}, u32[]{:S(2)}, u32[]{:S(2)}) %all-to-all-start.1) | async-done | bytes 1048608 | tf_op jit(solution)/shard_map/all_to_all | solution.py:40
  68.7 2.6 collective-permute-done
  71.3 0.7 convolution_convert_fusion.1
  72.3 0.7 convolution_convert_fusion
  73.4 0.6 convolution_convert_fusion.3
  75.4 18.5 %maximum_maximum_fusion = bf16[1024,2304]{1,0:T(8,128)(2,1)} fusion(bf16[256,1024]{1,0:T(8,128)(2,1)S(1)} %convolution_convert_fusion.4, bf16[256,1280]{1,0:T(8,128)(2,1)S(1)} %convolution_convert_fusion.2, bf16[256,768]{1,0:T(8,128)(2,1)S(1)} %convolution_convert_fusion.5, bf16[256,1536]{1,0:T(8,128)(2,1)S(1)} %convolution_convert_fusion.3, ...), kind=kLoop, calls=%fused_computation.49 | loop fusion | flops 37748736 | bytes 9437184 | tf_op jit(solution)/shard_map/concatenate | solution.py:71
  93.9 178.2 %all-reduce.3.cloned.1.call-done = bf16[1024,2304]{1,0:T(8,128)(2,1)} async-done(((bf16[1024,2304]{1,0:T(8,128)(2,1)}), bf16[1024,2304]{1,0:T(8,128)(2,1)}) %all-reduce.3.cloned.1.call-update) | async-done | bytes 4718608 | tf_op jit(solution)/shard_map/psum | solution.py:105
  272.1 1.4 fusion.67
  274.1 0.8 copy.176
  275.1 1.9 fusion.66
  277.0 0.8 copy.179
  277.8 0.7 copy.180
  278.5 0.8 copy.181
  279.3 0.8 copy.182
  280.1 0.8 copy.183
  280.8 0.8 copy.184
  283.0 1.3 slice_dynamic-update-slice_fusion
  284.4 1.2 slice.283
  285.7 1.2 slice.286
  287.1 1.1 slice.290
  288.4 1.1 slice_dynamic-update-slice_fusion.1
  289.7 1.0 slice_dynamic-update-slice_fusion.2
  290.8 1.0 slice_dynamic-update-slice_fusion.3
  291.9 0.9 slice_dynamic-update-slice_fusion.4
  292.9 3.2 copy-done.4
  296.1 4.9 fusion
  301.8 26.9 %fusion.5 = bf16[2048,2048]{1,0:T(8,128)(2,1)} fusion(f32[]{:T(128)S(6)} %div.3, bf16[2048,2048]{1,0:T(8,128)(2,1)} %copy-done.4), kind=kOutput, calls=%fused_computation.11 | convolution fusion | flops 17226006528 | bytes 16777220 | tf_op jit(solution)/shard_map/dot_general | solution.py:21
  328.7 21.5 %fusion.3 = bf16[2048,2048]{1,0:T(8,128)(2,1)} fusion(bf16[2048,2048]{1,0:T(8,128)(2,1)} %fusion.5, f32[]{:T(128)S(6)} %div.3, bf16[2048,2048]{1,0:T(8,128)(2,1)S(1)} %copy-done.5), kind=kOutput, calls=%fused_computation.9 | convolution fusion | flops 17221812224 | bytes 25165828 | tf_op jit(solution)/shard_map/dot_general | solution.py:21
  350.2 26.4 %add_convert_fusion.1 = bf16[2048,2048]{1,0:T(8,128)(2,1)} fusion(bf16[2048,2048]{1,0:T(8,128)(2,1)} %fusion.3, bf16[2048,2048]{1,0:T(8,128)(2,1)} %fusion.5), kind=kOutput, calls=%fused_computation.17 | convolution fusion | flops 17196646400 | bytes 25165824 | tf_op jit(solution)/shard_map/dot_general | solution.py:21
  376.6 26.6 %fusion.9 = bf16[2048,2048]{1,0:T(8,128)(2,1)} fusion(bf16[2048,2048]{1,0:T(8,128)(2,1)} %add_convert_fusion.1), kind=kOutput, calls=%fused_computation.15 | convolution fusion | flops 17200840704 | bytes 16777216 | tf_op jit(solution)/shard_map/dot_general | solution.py:21
  403.2 4.6 fusion.14
  407.8 5.4 %multiply_add_fusion.1 = f32[2048,512]{1,0:T(8,128)S(1)} fusion(f32[2048,512]{1,0:T(8,128)S(1)} %fusion.14, bf16[2048,2048]{1,0:T(8,128)(2,1)S(1)} %copy-done.5, f32[]{:T(128)S(6)} %div.3, f32[]{:T(128)S(6)} %sqrt.7, bf16[2048,256]{1,0:T(8,128)(2,1)S(1)} %copy-done.3, bf16[2048,256]{1,0:T(8,128)(2,1)S(1)} %copy-done.1), kind=kOutput, calls=%fused_computation.52 | convolution fusion | flops 4321181696 | bytes 18874376 | tf_op jit(solution)/shard_map/dot_general | solution.py:21
  413.2 7.6 %fusion.24 = f32[2048,512]{1,0:T(8,128)S(1)} fusion(bf16[2048,2048]{1,0:T(8,128)(2,1)} %add_convert_fusion.1, f32[2048,512]{1,0:T(8,128)S(1)} %multiply_add_fusion.1), kind=kOutput, calls=%fused_computation.67 | convolution fusion | flops 4296015872 | bytes 16777216 | tf_op jit(solution)/shard_map/dot_general | solution.py:21
  420.9 7.7 %multiply_add_fusion = f32[2048,512]{1,0:T(8,128)S(1)} fusion(f32[2048,512]{1,0:T(8,128)S(1)} %fusion.24, f32[2048,512]{1,0:T(8,128)S(1)} %multiply_add_fusion.1, bf16[2048,2048]{1,0:T(8,128)(2,1)} %add_convert_fusion.1), kind=kOutput, calls=%fused_computation.51 | convolution fusion | flops 4301258752 | bytes 20971520 | tf_op jit(solution)/shard_map/dot_general | solution.py:21
  428.6 20.1 %fusion.7 = bf16[2048,2048]{1,0:T(8,128)(2,1)S(1)} fusion(bf16[2048,2048]{1,0:T(8,128)(2,1)S(1)} %bitcast.115, bf16[2048,2048]{1,0:T(8,128)(2,1)} %fusion.9), kind=kOutput, calls=%fused_computation.13 | convolution fusion | flops 17196646400 | bytes 25165824 | tf_op jit(solution)/shard_map/dot_general | solution.py:21
  448.7 20.3 %add_convert_fusion = bf16[2048,2048]{1,0:T(8,128)(2,1)S(1)} fusion(bf16[2048,2048]{1,0:T(8,128)(2,1)S(1)} %fusion.7, bf16[2048,2048]{1,0:T(8,128)(2,1)} %fusion.9), kind=kOutput, calls=%fused_computation.16 | convolution fusion | flops 17196646400 | bytes 25165824 | tf_op jit(solution)/shard_map/dot_general | solution.py:21
  469.0 4.5 fusion.21
  473.6 6.0 %add_convert_fusion.2 = bf16[2048,512]{1,0:T(8,128)(2,1)S(1)} fusion(f32[2048,512]{1,0:T(8,128)S(1)} %fusion.21, f32[2048,512]{1,0:T(8,128)S(1)} %multiply_add_fusion, bf16[2048,2048]{1,0:T(8,128)(2,1)S(1)} %add_convert_fusion), kind=kOutput, calls=%fused_computation.50 | convolution fusion | flops 4302307328 | bytes 18874368 | tf_op jit(solution)/shard_map/dot_general | solution.py:21
  479.8 2.6 collective-permute-done.1
  482.4 1.1 fusion.68
  483.8 11.9 %all_to_all.30 = bf16[4,512,64]{1,2,0:T(8,128)(2,1)S(1)} all-to-all(bf16[4,512,64]{1,2,0:T(8,128)(2,1)S(1)} %copy.164), channel_id=1, replica_groups=mesh['fs'=4,'tp'=4,'rep'=2] {'fs'}, dimensions={0} | all-to-all | bytes 524288 | tf_op jit(solution)/shard_map/all_to_all | solution.py:48
  495.7 3.5 all-to-all-start.4
  499.2 1.0 copy.165
  500.2 0.9 convert_multiply_fusion.8
  501.1 2.0 bitcast_subtract_fusion
  503.1 2.0 copy.166
  505.2 2.0 copy.167
  507.2 16.5 %all-to-all-done.4 = bf16[4,512,256]{2,1,0:T(8,128)(2,1)S(1)} async-done(((bf16[4,512,256]{2,1,0:T(8,128)(2,1)}), bf16[4,512,256]{2,1,0:T(8,128)(2,1)S(1)}, u32[]{:S(2)}, u32[]{:S(2)}) %all-to-all-start.4) | async-done | bytes 1048608 | tf_op jit(solution)/shard_map/all_to_all | solution.py:48
  524.4 1.6 copy.200
  526.1 1.7 sub.6
  (101 shorter events, 7.1 us)
Async XLA Ops:
  7.2 14.9 %copy-start.7 = (f32[512,256]{1,0:T(8,128)S(1)}, f32[512,256]{1,0:T(8,128)}, u32[]{:S(2)}) copy-start(f32[512,256]{1,0:T(8,128)} %param.10) | copy-start | bytes 1572868
  9.5 8.8 %all-to-all-start.2 = ((bf16[2,512,256]{2,1,0:T(8,128)(2,1)}), bf16[2,512,256]{2,1,0:T(8,128)(2,1)S(1)}, u32[]{:S(2)}, u32[]{:S(2)}) async-start(bf16[2,512,256]{2,1,0:T(8,128)(2,1)} %copy.129), calls=%async_computation.2 | async-start | bytes 1048576 | tf_op jit(solution)/shard_map/all_to_all | solution.py:32
  18.2 6.6 %all-to-all-start = ((bf16[2,512,1024]{2,1,0:T(8,128)(2,1)}), bf16[2,512,1024]{2,1,0:T(8,128)(2,1)S(1)}, u32[]{:S(2)}, u32[]{:S(2)}) async-start(bf16[2,512,1024]{2,1,0:T(8,128)(2,1)} %copy.126), calls=%async_computation | async-start | bytes 4194304 | tf_op jit(solution)/shard_map/all_to_all | solution.py:32
  24.9 15.6 %all-to-all-start.3 = ((bf16[4,512,64]{1,2,0:T(8,128)(2,1)}), bf16[4,512,64]{1,2,0:T(8,128)(2,1)S(1)}, u32[]{:S(2)}, u32[]{:S(2)}) async-start(bf16[4,512,64]{1,2,0:T(8,128)(2,1)} %bitcast.7), calls=%async_computation.3 | async-start | bytes 524288 | tf_op jit(solution)/shard_map/all_to_all | solution.py:40
  40.4 27.7 %all-to-all-start.1 = ((bf16[4,512,256]{2,1,0:T(8,128)(2,1)}), bf16[4,512,256]{2,1,0:T(8,128)(2,1)S(1)}, u32[]{:S(2)}, u32[]{:S(2)}) async-start(bf16[4,512,256]{2,1,0:T(8,128)(2,1)} %bitcast.99), calls=%async_computation.1 | async-start | bytes 2097152 | tf_op jit(solution)/shard_map/all_to_all | solution.py:40
  44.0 228.1 %all-reduce.3.cloned.1.call-start = ((), (), s32[]{:S(2)}) async-start(), calls=%async_computation.6 | async-start | bytes 9437184 | tf_op jit(solution)/shard_map/psum | solution.py:105
  68.6 6.3 %copy-start = (bf16[2048,256]{1,0:T(8,128)(2,1)}, bf16[2048,256]{1,0:T(8,128)(2,1)S(1)}, u32[]{:S(2)}) copy-start(bf16[2048,256]{1,0:T(8,128)(2,1)S(1)} %get-tuple-element.59) | copy-start | bytes 3145732
  68.6 2.7 collective-permute-start
  71.3 3.6 copy-start.2
  280.8 7.5 %copy-start.9 = (bf16[256,256]{0,1:T(8,128)(2,1)S(1)}, bf16[256,256]{0,1:T(8,128)(2,1)}, u32[]{:S(2)}) copy-start(bf16[256,256]{0,1:T(8,128)(2,1)} %copy.176) | copy-start | bytes 393220
  282.4 7.1 %copy-start.13 = (bf16[256,256]{0,1:T(8,128)(2,1)S(1)}, bf16[256,256]{0,1:T(8,128)(2,1)}, u32[]{:S(2)}) copy-start(bf16[256,256]{0,1:T(8,128)(2,1)} %copy.181) | copy-start | bytes 393220
  282.6 7.0 %copy-start.12 = (bf16[256,256]{0,1:T(8,128)(2,1)S(1)}, bf16[256,256]{0,1:T(8,128)(2,1)}, u32[]{:S(2)}) copy-start(bf16[256,256]{0,1:T(8,128)(2,1)} %copy.182) | copy-start | bytes 393220
  282.7 6.9 %copy-start.11 = (bf16[256,256]{0,1:T(8,128)(2,1)S(1)}, bf16[256,256]{0,1:T(8,128)(2,1)}, u32[]{:S(2)}) copy-start(bf16[256,256]{0,1:T(8,128)(2,1)} %copy.183) | copy-start | bytes 393220
  282.8 6.8 %copy-start.10 = (bf16[256,256]{0,1:T(8,128)(2,1)S(1)}, bf16[256,256]{0,1:T(8,128)(2,1)}, u32[]{:S(2)}) copy-start(bf16[256,256]{0,1:T(8,128)(2,1)} %copy.184) | copy-start | bytes 393220
  283.0 5.4 %copy-start.15 = (bf16[256,256]{0,1:T(8,128)(2,1)S(1)}, bf16[256,256]{0,1:T(8,128)(2,1)}, u32[]{:S(2)}) copy-start(bf16[256,256]{0,1:T(8,128)(2,1)} %copy.179) | copy-start | bytes 393220
  283.0 6.5 %copy-start.14 = (bf16[256,256]{0,1:T(8,128)(2,1)S(1)}, bf16[256,256]{0,1:T(8,128)(2,1)}, u32[]{:S(2)}) copy-start(bf16[256,256]{0,1:T(8,128)(2,1)} %copy.180) | copy-start | bytes 393220
  292.8 3.2 copy-start.4
  301.8 26.9 %copy-start.5 = (bf16[2048,2048]{1,0:T(8,128)(2,1)S(1)}, bf16[2048,2048]{1,0:T(8,128)(2,1)}, u32[]{:S(2)}) copy-start(bf16[2048,2048]{1,0:T(8,128)(2,1)} %copy-done.4) | copy-start | bytes 25165828
  376.6 26.6 %copy-start.1 = (bf16[2048,256]{1,0:T(8,128)(2,1)S(1)}, bf16[2048,256]{1,0:T(8,128)(2,1)}, u32[]{:S(2)}) copy-start(bf16[2048,256]{1,0:T(8,128)(2,1)} %copy-done) | copy-start | bytes 3145732
  376.6 26.6 %copy-start.3 = (bf16[2048,256]{1,0:T(8,128)(2,1)S(1)}, bf16[2048,256]{1,0:T(8,128)(2,1)}, u32[]{:S(2)}) copy-start(bf16[2048,256]{1,0:T(8,128)(2,1)} %copy-done.2) | copy-start | bytes 3145732
  413.2 15.4 %slice-start = ((s8[8388608]{0:T(1024)(128)(4,1)}), s8[4194304]{0:T(1024)(128)(4,1)S(1)}, s32[]{:S(2)}) async-start(s8[8388608]{0:T(1024)(128)(4,1)} %bitcast.114), calls=%async_computation.7 | async-start | bytes 8388608
  420.8 7.8 %slice-start.1 = ((s8[8388608]{0:T(1024)(128)(4,1)}), s8[4194304]{0:T(1024)(128)(4,1)S(1)}, s32[]{:S(2)}) async-start(s8[8388608]{0:T(1024)(128)(4,1)} %bitcast.114), calls=%async_computation.8 | async-start | bytes 8388608
  479.6 19.6 %copy-start.8 = (f32[512,256]{1,0:T(8,128)S(1)}, f32[512,256]{1,0:T(8,128)}, u32[]{:S(2)}) copy-start(f32[512,256]{1,0:T(8,128)} %param.9) | copy-start | bytes 1572868
  479.7 2.7 collective-permute-start.1
  495.7 28.0 %all-to-all-start.4 = ((bf16[4,512,256]{2,1,0:T(8,128)(2,1)}), bf16[4,512,256]{2,1,0:T(8,128)(2,1)S(1)}, u32[]{:S(2)}, u32[]{:S(2)}) async-start(bf16[4,512,256]{2,1,0:T(8,128)(2,1)} %bitcast.37), calls=%async_computation.4 | async-start | bytes 2097152 | tf_op jit(solution)/shard_map/all_to_all | solution.py:48
  501.1 25.0 %copy-start.6 = (f32[512,1024]{1,0:T(8,128)S(1)}, f32[512,1024]{1,0:T(8,128)}, u32[]{:S(2)}) copy-start(f32[512,1024]{1,0:T(8,128)} %param.6) | copy-start | bytes 6291460
Sparse Core Ops, SparseCore 0:
  94.0 178.0 all-reduce.2
where the time goes:
time: 541 us; the launch traced here: 535 us
  waiting for transfers between devices  229 us (42%)
  matrix products  182 us (34%)
  local copies, waits for them, and re-layouts  40.1 us (7%)
  other arithmetic  35.2 us (7%)
  starting transfers between devices  20.8 us (4%)
  between operations  16 us (3%)
  blocking collectives  11.9 us (2%)
    psum x1, waiting for transfers between devices, on_device(): lax.psum(pack_gram(values), ('fs', 'tp'))  178 us
    dot_general x12, matrix products, mm(): return jnp.dot(a, b, preferred_element_type=F32)  178 us
    all_to_all x2, waiting for transfers between devices, to_columns(): lax.all_to_all(pieces, 'fs', split_axis=0, concat_axis=0, tiled=True)  28.1 us
    unnamed x95, local copies, waits for them, and re-layouts  24.6 us
    concatenate x1, other arithmetic, pack_gram(): return jnp.concatenate(rows, axis=0)  18.5 us
    all_to_all x1, waiting for transfers between devices, to_rows(): lax.all_to_all(pieces, 'fs', split_axis=0, concat_axis=0, tiled=True)  16.5 us
    all_to_all x1, blocking collectives, to_rows(): lax.all_to_all(pieces, 'fs', split_axis=0, concat_axis=0, tiled=True)  11.9 us
  transfers between devices with their start and end apart: 8, of which 7 were waited for; matrix products, arithmetic and copies ran while one was open for 4% of the time, Pallas kernels for 0%

commit v1 on v0

v1 whole, which is shorter than its diff:
```python
import functools
import math

import jax
import jax.numpy as jnp
from jax import lax
from jax.experimental import pallas as pl
from jax.experimental.pallas import tpu as pltpu
from jax.sharding import PartitionSpec as P

ITERS = 3
MOMENT = 0.9
RATE = 0.02
COEF_A = 3.4445
COEF_B = -4.775
COEF_C = 2.0315
BF = jnp.bfloat16
F32 = jnp.float32
CUTS = 8
PANELS = 4


def mm(a, b):
    return jnp.dot(a, b, preferred_element_type=F32)


def mm_t(a, b):
    return lax.dot_general(a, b, (((1,), (1,)), ((), ())), preferred_element_type=F32)


def reduced_grad(grads):
    size = lax.axis_size("rep")
    rows, cols = grads.shape
    pieces = grads.reshape(rows, size, cols // size).transpose(1, 0, 2)
    pieces = lax.all_to_all(pieces, "rep", split_axis=0, concat_axis=0, tiled=True)
    return jnp.sum(pieces.astype(F32), axis=0)


def to_columns(values):
    size = lax.axis_size("fs")
    rows, cols = values.shape
    pieces = values.reshape(rows, size, cols // size).transpose(1, 0, 2)
    pieces = lax.all_to_all(pieces, "fs", split_axis=0, concat_axis=0, tiled=True)
    return pieces.reshape(size * rows, cols // size)


def to_rows(values):
    size = lax.axis_size("fs")
    rows, cols = values.shape
    pieces = values.reshape(size, rows // size, cols)
    pieces = lax.all_to_all(pieces, "fs", split_axis=0, concat_axis=0, tiled=True)
    return pieces.transpose(1, 0, 2).reshape(rows // size, cols * size)


def swap_pairs(values):
    size = lax.axis_size("rep")
    return lax.ppermute(values, "rep", [(i, i ^ 1) for i in range(size)])


def blocks_of(cuts):
    return [(i, j) for i in range(cuts) for j in range(i, cuts)]


def gram_kernel(x_ref, o_ref):
    step = x_ref.shape[0] // CUTS
    span = CUTS // PANELS
    place = {pair: k for k, pair in enumerate(blocks_of(CUTS))}
    for p in range(PANELS):
        low = p * span
        rows = x_ref[low * step : (low + span) * step, :]
        value = mm_t(rows, x_ref[low * step :, :]).astype(BF)
        for i in range(span):
            for j in range(low + i, CUTS):
                k = place[low + i, j]
                o_ref[k * step : (k + 1) * step, :] = value[
                    i * step : (i + 1) * step, (j - low) * step : (j - low + 1) * step
                ]


def gram(x):
    size, width = x.shape
    step = size // CUTS
    count = len(blocks_of(CUTS))
    return pl.pallas_call(
        gram_kernel,
        name="gram",
        out_shape=jax.ShapeDtypeStruct((count * step, step), BF),
        in_specs=[pl.BlockSpec(memory_space=pltpu.VMEM)],
        out_specs=pl.BlockSpec(memory_space=pltpu.VMEM),
        compiler_params=pltpu.CompilerParams(vmem_limit_bytes=48 << 20),
        cost_estimate=pl.CostEstimate(
            flops=2 * width * count * step * step, bytes_accessed=2 * size * width, transcendentals=0
        ),
    )(x)


S1X, S1Y, S2X0, S2X1, S2Y0, S2Y1, RZ, AZ, AX, AY, AD0, AD1 = range(12)


def reduce_kernel(planes, g_ref, o_ref, first, second, mixed, third, moved, own, send, recv):
    z, t, r = lax.axis_index("fs"), lax.axis_index("tp"), lax.axis_index("rep")
    half = g_ref.shape[1] // 2
    parts = (pl.ds(0, half), pl.ds(half, half))
    beside, above, corner = t ^ 1, t ^ 2, t ^ 3
    to_x, to_y = (z, beside, r), (z, above, r)
    others = list(range(1, planes))
    order = others + [0]

    barrier = pltpu.get_barrier_semaphore()
    peers = [to_x, to_y] + [(z ^ m, t, r) for m in others]
    for peer in peers:
        pl.semaphore_signal(barrier, inc=1, device_id=peer, device_id_type=pl.DeviceIdType.MESH)
    pl.semaphore_wait(barrier, len(peers))

    def chunk(m, s):
        return (z ^ m) * 4 + s

    started = []

    def copy(kind, m, src, dst, peer, start=True):
        c = pltpu.make_async_remote_copy(
            src_ref=src,
            dst_ref=dst,
            send_sem=send.at[kind, m],
            recv_sem=recv.at[kind, m],
            device_id=peer,
            device_id_type=pl.DeviceIdType.MESH,
        )
        if start:
            c.start()
            started.append(c)
        return c

    def arrived(kind, m, dst):
        copy(kind, m, dst, dst, to_x, start=False).wait_recv()

    def corner_halves(m):
        copy(S1Y, m, g_ref.at[chunk(m, corner), parts[0]], first.at[m, 0], to_y)
        copy(S1X, m, g_ref.at[chunk(m, corner), parts[1]], first.at[m, 1], to_x)

    def direct_halves(m):
        copy(S2X1, m, g_ref.at[chunk(m, beside), parts[1]], second.at[m, 0, parts[1]], to_x)
        copy(S2Y0, m, g_ref.at[chunk(m, above), parts[0]], second.at[m, 1, parts[0]], to_y)

    corner_halves(order[0])
    corner_halves(order[1])
    direct_halves(order[0])
    for k in range(planes + 1):
        if k < planes:
            m = order[k]
            arrived(S1Y, m, first.at[m, 0])
            mixed[m, 0] = (g_ref[chunk(m, beside), parts[0]].astype(F32) + first[m, 0].astype(F32)).astype(BF)
            copy(S2X0, m, mixed.at[m, 0], second.at[m, 0, parts[0]], to_x)
            arrived(S1X, m, first.at[m, 1])
            mixed[m, 1] = (g_ref[chunk(m, above), parts[1]].astype(F32) + first[m, 1].astype(F32)).astype(BF)
            copy(S2Y1, m, mixed.at[m, 1], second.at[m, 1, parts[1]], to_y)
            if k + 2 < planes:
                corner_halves(order[k + 2])
            if k + 1 < planes:
                direct_halves(order[k + 1])
        if k >= 1:
            m = order[k - 1]
            arrived(S2X1, m, second.at[m, 0, parts[1]])
            arrived(S2Y0, m, second.at[m, 1, parts[0]])
            arrived(S2X0, m, second.at[m, 0, parts[0]])
            arrived(S2Y1, m, second.at[m, 1, parts[1]])
            value = g_ref[chunk(m, t)].astype(F32) + second[m, 0].astype(F32) + second[m, 1].astype(F32)
            if m:
                moved[m] = value.astype(BF)
                copy(RZ, m, moved.at[m], third.at[m], (z ^ m, t, r))
            else:
                own[...] = value
    value = own[...]
    for m in others:
        arrived(RZ, m, third.at[m])
        value = value + third[m].astype(F32)
    o_ref[chunk(0, t)] = value.astype(BF)

    def to_neighbours(m):
        copy(AX, m, o_ref.at[chunk(m, t)], o_ref.at[chunk(m, t)], to_x)
        copy(AY, m, o_ref.at[chunk(m, t)], o_ref.at[chunk(m, t)], to_y)

    def to_corner(m):
        arrived(AX, m, o_ref.at[chunk(m, beside)])
        copy(AD0, m, o_ref.at[chunk(m, beside), parts[0]], o_ref.at[chunk(m, beside), parts[0]], to_y)
        arrived(AY, m, o_ref.at[chunk(m, above)])
        copy(AD1, m, o_ref.at[chunk(m, above), parts[1]], o_ref.at[chunk(m, above), parts[1]], to_x)

    to_neighbours(0)
    for m in others:
        copy(AZ, m, o_ref.at[chunk(0, t)], o_ref.at[chunk(0, t)], (z ^ m, t, r))
    before = 0
    for m in others:
        arrived(AZ, m, o_ref.at[chunk(m, t)])
        to_neighbours(m)
        to_corner(before)
        before = m
    to_corner(before)
    for m in [0] + others:
        arrived(AD0, m, o_ref.at[chunk(m, corner), parts[0]])
        arrived(AD1, m, o_ref.at[chunk(m, corner), parts[1]])
    for c in started:
        c.wait_send()


def reduced(packed):
    planes = lax.axis_size("fs")
    chunks = planes * 4
    rows, width = packed.shape
    size = rows // chunks
    out = pl.pallas_call(
        functools.partial(reduce_kernel, planes),
        name="reduced",
        out_shape=jax.ShapeDtypeStruct((chunks, size, width), BF),
        in_specs=[pl.BlockSpec(memory_space=pltpu.VMEM)],
        out_specs=pl.BlockSpec(memory_space=pltpu.VMEM),
        scratch_shapes=[
            pltpu.VMEM((planes, 2, size // 2, width), BF),
            pltpu.VMEM((planes, 2, size, width), BF),
            pltpu.VMEM((planes, 2, size // 2, width), BF),
            pltpu.VMEM((planes, size, width), BF),
            pltpu.VMEM((planes, size, width), BF),
            pltpu.VMEM((size, width), F32),
            pltpu.SemaphoreType.DMA((12, planes)),
            pltpu.SemaphoreType.DMA((12, planes)),
        ],
        compiler_params=pltpu.CompilerParams(
            collective_id=1, has_side_effects=True, vmem_limit_bytes=48 << 20
        ),
    )(packed.reshape(chunks, size, width))
    return out.reshape(rows, width)


def total_gram(packed):
    fs, tp, rep = (lax.axis_size(name) for name in ("fs", "tp", "rep"))
    if rep == 2 and tp == 4 and fs & (fs - 1) == 0 and packed.shape[0] % (fs * tp * 32) == 0:
        return reduced(packed)
    packed = lax.psum(packed, ("fs", "tp"))
    if rep > 2:
        groups = [[i for i in range(rep) if i % 2 == k] for k in range(2)]
        packed = lax.psum(packed, "rep", axis_index_groups=groups)
    return packed


def unpack(packed, mats):
    step = packed.shape[1]
    pairs = blocks_of(CUTS)
    total = jnp.zeros((step, step), F32)
    for k, (i, j) in enumerate(pairs):
        value = packed[k * step : (k + 1) * step, :].astype(F32)
        total = total + (value * value if i == j else 2.0 * (value * value))
    square = 1.0 / (jnp.sqrt(jnp.sum(total, keepdims=True)) + 1.0)
    for k, (i, j) in enumerate(pairs):
        value = (packed[k * step : (k + 1) * step, :].astype(F32) * square).astype(BF)
        mats[0, i * step : (i + 1) * step, j * step : (j + 1) * step] = value
        if i != j:
            mats[0, j * step : (j + 1) * step, i * step : (i + 1) * step] = value.T
    return jnp.sqrt(square)


def symmetric_step(mats, left, right, out, alpha, beta):
    size = mats.shape[1]
    step = size // PANELS
    for i in range(PANELS):
        low, high = i * step, (i + 1) * step
        product = mm(mats[left, low:high, :], mats[right, :, low:])
        value = (alpha * mats[right, low:high, low:].astype(F32) + beta * product).astype(BF)
        mats[out, low:high, low:] = value
        for j in range(i + 1, PANELS):
            mats[out, j * step : (j + 1) * step, low:high] = value[:, (j - i) * step : (j - i + 1) * step].T


def thin_step(mats, index, vals, source, target, alpha):
    size = mats.shape[1]
    step = size // PANELS

    def panel(i, _):
        rows = pl.ds(pl.multiple_of(i * step, step), step)
        product = mm(mats[index, rows, :], vals[source])
        vals[target, rows, :] = (alpha * vals[source, rows, :].astype(F32) + product).astype(BF)
        return 0

    lax.fori_loop(0, PANELS, panel, 0)


def chain_kernel(g_ref, v_ref, o_ref, mats, vals):
    factor = unpack(g_ref, mats)
    vals[0] = v_ref[...]

    def product(k, _):
        left = jnp.where(k == 0, 0, 1)
        right = jnp.where(k == 2, 2, 0)
        out = jnp.where(k == 0, 1, jnp.where(k == 1, 2, 0))
        alpha = jnp.where(k == 0, COEF_B, COEF_A).astype(F32)
        beta = jnp.where(k == 0, COEF_C, 1.0).astype(F32)
        symmetric_step(mats, left, right, out, alpha, beta)
        return 0

    def iteration(t, _):
        lax.fori_loop(0, 3, product, 0)
        thin_step(mats, 1, vals, t, t + 1, COEF_A)
        return 0

    lax.fori_loop(0, ITERS - 1, iteration, 0)
    size = mats.shape[1]
    step = size // PANELS
    last = ITERS - 1
    for source, target in ((last, 0), (0, 1)):
        def panel(i, _):
            rows = pl.ds(pl.multiple_of(i * step, step), step)
            product = mm(mats[0, rows, :], vals[source])
            if target == 0:
                vals[0, rows, :] = product.astype(BF)
            else:
                value = COEF_A * vals[last, rows, :].astype(F32) + COEF_B * vals[0, rows, :].astype(F32)
                o_ref[rows, :] = (factor * (value + COEF_C * product)).astype(BF)
            return 0
        lax.fori_loop(0, PANELS, panel, 0)


def chain(packed, v):
    size, width = v.shape
    flops = 2 * size * size * (4 * width + 6 * size * 5 // 8)
    return pl.pallas_call(
        chain_kernel,
        name="chain",
        out_shape=jax.ShapeDtypeStruct(v.shape, BF),
        in_specs=[pl.BlockSpec(memory_space=pltpu.VMEM)] * 2,
        out_specs=pl.BlockSpec(memory_space=pltpu.VMEM),
        scratch_shapes=[pltpu.VMEM((3, size, size), BF), pltpu.VMEM((ITERS, size, width), BF)],
        compiler_params=pltpu.CompilerParams(vmem_limit_bytes=60 << 20),
        cost_estimate=pl.CostEstimate(flops=flops, bytes_accessed=2 * size * (size + 2 * width), transcendentals=0),
    )(packed, v)


def on_device(up_weight, up_momentum, up_grads, out_weight, out_momentum, out_grads):
    even = lax.axis_index("rep") % 2 == 0
    up_moment = MOMENT * up_momentum + reduced_grad(up_grads[0])
    out_moment = MOMENT * out_momentum + reduced_grad(out_grads[0])
    up = to_columns(up_moment.astype(BF))
    out = to_columns(out_moment.astype(BF))
    width, narrow = up.shape[1], out.shape[1]
    out = jnp.pad(out, ((0, 0), (0, width - narrow)))
    other = swap_pairs(jnp.where(even, out, up))
    values = jnp.concatenate([jnp.where(even, up, out), other], axis=1)
    final = chain(total_gram(gram(values)), values)
    mine, other = final[:, :width], swap_pairs(final[:, width:])
    up = to_rows(jnp.where(even, mine, other)).astype(F32)
    out = to_rows(jnp.where(even, other, mine)[:, :narrow]).astype(F32)
    group = lax.axis_size("tp") * lax.axis_size("rep")
    up_direction = up * math.sqrt(up_weight.shape[1] * group)
    out_direction = out * math.sqrt(out_weight.shape[1] * group)
    return (
        up_weight - RATE * up_direction,
        up_moment,
        up_direction,
        out_weight - RATE * out_direction,
        out_moment,
        out_direction,
    )


def solution(mesh):
    flat = P("fs", ("tp", "rep"))
    grads = P("rep", "fs", "tp")
    return jax.shard_map(
        on_device,
        mesh=mesh,
        in_specs=(flat, flat, grads, flat, flat, grads),
        out_specs=(flat,) * 6,
        check_vma=False,
    )
```

time: 541 us -> 334 us (0.62)
  Pallas kernels: 0 us -> 215 us
  matrix products: 182 us -> 0 us
  waiting for transfers between devices: 229 us -> 57.7 us
  other arithmetic: 35.2 us -> 7.23 us
  local copies, waits for them, and re-layouts: 40.1 us -> 19.4 us
  between operations: 16 us -> 0.85 us
    pallas_call x0 -> x3, Pallas kernels: none -> 215 us  [the longest x1 106 us: chain(): pl.pallas_call(chain_kernel, name='chain', out_shape=jax.ShapeDtypeStruct...]
    dot_general x20 -> x0, matrix products: 182 us -> none  [the longest x12 178 us: mm(): return jnp.dot(a, b, preferred_element_type=F32)]
    psum x1 -> x0, waiting for transfers between devices: 178 us -> none  [on_device(): lax.psum(pack_gram(values), ('fs', 'tp'))]
    concatenate x1, other arithmetic: 18.5 us -> 0.16 us  [on_device(): values = jnp.concatenate([jnp.where(even, up, out), other], axis=1)]
    unnamed x95 -> x19, local copies, waits for them, and re-layouts: 24.6 us -> 10.3 us
    slice x5 -> x0, local copies, waits for them, and re-layouts: 6.91 us -> none  [the longest x3 3.57 us: unpack_gram(): upper[i] = row[:, :(CUTS - i) * step]]
    all_to_all x1, waiting for transfers between devices: 16.5 us -> 22.7 us  [to_rows(): lax.all_to_all(pieces, 'fs', split_axis=0, concat_axis=0, tiled=True)]
  transfers between devices with their start and end apart: 8 -> 7, of which waited for: 7 -> 6; matrix products, arithmetic and copies ran while one was open for 4% -> 4% of each run, Pallas kernels for 0% -> 0%
where the time goes in v1:
time: 334 us; the launch traced here: 333 us
  Pallas kernels  215 us (64%)
  waiting for transfers between devices  57.7 us (17%)
  starting transfers between devices  20.9 us (6%)
  local copies, waits for them, and re-layouts  19.4 us (6%)
  blocking collectives  11.8 us (4%)
  other arithmetic  7.23 us (2%)
    pallas_call x1, Pallas kernels, chain(): pl.pallas_call(chain_kernel, name='chain', out_shape=jax.ShapeDtypeStruct...  106 us
    pallas_call x1, Pallas kernels, reduced(): pl.pallas_call(functools.partial(reduce_kernel, planes), name='reduced',...  104 us
    all_to_all x2, waiting for transfers between devices, to_columns(): lax.all_to_all(pieces, 'fs', split_axis=0, concat_axis=0, tiled=True)  28.7 us
    all_to_all x1, waiting for transfers between devices, to_rows(): lax.all_to_all(pieces, 'fs', split_axis=0, concat_axis=0, tiled=True)  22.7 us
    all_to_all x1, blocking collectives, to_rows(): lax.all_to_all(pieces, 'fs', split_axis=0, concat_axis=0, tiled=True)  11.8 us
    unnamed x19, local copies, waits for them, and re-layouts  10.3 us
    all_to_all x2, starting transfers between devices, to_columns(): lax.all_to_all(pieces, 'fs', split_axis=0, concat_axis=0, tiled=True)  9.86 us
    all_to_all x2, starting transfers between devices, reduced_grad(): lax.all_to_all(pieces, 'rep', split_axis=0, concat_axis=0, tiled=True)  7.39 us
  transfers between devices with their start and end apart: 7, of which 6 were waited for; matrix products, arithmetic and copies ran while one was open for 4% of the time, Pallas kernels for 0%

profile of v1, /device:TPU:0, one launch (start us, length us, event | category | flops | bytes accessed | tf_op | source)
XLA Modules:
  0.0 332.9 jit_solution(1680587420189534249)
XLA Ops:
  0.6 1.3 copy.41
  1.9 1.0 copy.42
  2.9 3.5 %all-to-all-start.2 = ((bf16[2,512,256]{2,1,0:T(8,128)(2,1)}), bf16[2,512,256]{2,1,0:T(8,128)(2,1)S(1)}, u32[]{:S(2)}, u32[]{:S(2)}) async-start(bf16[2,512,256]{2,1,0:T(8,128)(2,1)} %copy.42), calls=%async_computation.2 | async-start | bytes 1048576 | tf_op jit(solution)/shard_map/all_to_all | solution.py:35
  6.4 2.9 copy.38
  9.3 2.4 copy.39
  11.6 0.0 copy-start.5
  11.6 0.0 all-to-all-done.2
  11.6 3.9 %all-to-all-start = ((bf16[2,512,1024]{2,1,0:T(8,128)(2,1)}), bf16[2,512,1024]{2,1,0:T(8,128)(2,1)S(1)}, u32[]{:S(2)}, u32[]{:S(2)}) async-start(bf16[2,512,1024]{2,1,0:T(8,128)(2,1)} %copy.39), calls=%async_computation | async-start | bytes 4194304 | tf_op jit(solution)/shard_map/all_to_all | solution.py:35
  15.6 0.1 convert_reduce_fusion.1
  15.6 0.0 copy-done.5
  15.6 0.9 fusion.3
  16.5 0.8 copy.44
  17.3 1.1 all-to-all-done
  18.4 6.3 %all-to-all-start.3 = ((bf16[4,512,64]{1,2,0:T(8,128)(2,1)}), bf16[4,512,64]{1,2,0:T(8,128)(2,1)S(1)}, u32[]{:S(2)}, u32[]{:S(2)}) async-start(bf16[4,512,64]{1,2,0:T(8,128)(2,1)} %bitcast.7), calls=%async_computation.3 | async-start | bytes 524288 | tf_op jit(solution)/shard_map/all_to_all | solution.py:43
  24.8 0.0 copy-start.2
  24.8 0.4 convert_reduce_fusion
  25.2 1.1 copy-done.2
  26.3 1.8 fusion.2
  28.2 1.0 copy.57
  29.2 4.7 %all-to-all-done.3 = bf16[4,512,64]{1,2,0:T(8,128)(2,1)S(1)} async-done(((bf16[4,512,64]{1,2,0:T(8,128)(2,1)}), bf16[4,512,64]{1,2,0:T(8,128)(2,1)S(1)}, u32[]{:S(2)}, u32[]{:S(2)}) %all-to-all-start.3) | async-done | bytes 262176 | tf_op jit(solution)/shard_map/all_to_all | solution.py:43
  34.0 3.5 %all-to-all-start.1 = ((bf16[4,512,256]{2,1,0:T(8,128)(2,1)}), bf16[4,512,256]{2,1,0:T(8,128)(2,1)S(1)}, u32[]{:S(2)}, u32[]{:S(2)}) async-start(bf16[4,512,256]{2,1,0:T(8,128)(2,1)} %bitcast.38), calls=%async_computation.1 | async-start | bytes 2097152 | tf_op jit(solution)/shard_map/all_to_all | solution.py:43
  37.5 0.3 copy.45
  37.8 23.9 %all-to-all-done.1 = bf16[4,512,256]{2,1,0:T(8,128)(2,1)S(1)} async-done(((bf16[4,512,256]{2,1,0:T(8,128)(2,1)}), bf16[4,512,256]{2,1,0:T(8,128)(2,1)S(1)}, u32[]{:S(2)}, u32[]{:S(2)}) %all-to-all-start.1) | async-done | bytes 1048608 | tf_op jit(solution)/shard_map/all_to_all | solution.py:43
  61.7 0.4 pad_select_fusion.1
  62.1 0.1 collective-permute-start
  62.2 2.6 collective-permute-done
  64.8 0.2 pad_maximum_fusion.x_ref.v_ref
  65.0 0.0 copy-start.1
  65.0 5.0 %gram.1 = bf16[9216,256]{1,0:T(8,128)(2,1)} custom-call(bf16[2048,512]{1,0:T(8,128)(2,1)S(1)} %pad_maximum_fusion.x_ref.v_ref), custom_call_target="tpu_custom_call" | custom-call | flops 2415919104 | bytes 2097152 | tf_op jit(solution)/shard_map/gram/pallas_call | solution.py:84
  70.1 0.0 copy-done.1
  70.1 104.3 %reduced.1 = bf16[16,576,256]{2,1,0:T(8,128)(2,1)S(1)} custom-call(bf16[16,576,256]{2,1,0:T(8,128)(2,1)} %bitcast.42), custom_call_target="tpu_custom_call" | custom-call | tf_op jit(solution)/shard_map/reduced/pallas_call | solution.py:211
  174.3 0.0 copy-start
  174.3 2.1 copy-done
  176.5 105.7 %chain.1 = bf16[2048,512]{1,0:T(8,128)(2,1)} custom-call(bf16[9216,256]{1,0:T(8,128)(2,1)} %bitcast.39, bf16[2048,512]{1,0:T(8,128)(2,1)} %copy-done.1), custom_call_target="tpu_custom_call" | custom-call | flops 81604378624 | bytes 12582912 | tf_op jit(solution)/shard_map/chain/pallas_call | solution.py:324
  282.1 0.0 copy-start.4
  282.1 1.4 slice.13
  283.6 0.1 collective-permute-start.1
  283.7 2.6 collective-permute-done.1
  286.3 0.0 copy-done.4
  286.3 1.1 fusion.4
  287.4 0.1 slice_select_fusion
  287.5 0.0 copy-start.6
  287.5 0.2 copy.48
  287.7 11.8 %all_to_all.30 = bf16[4,512,64]{1,2,0:T(8,128)(2,1)S(1)} all-to-all(bf16[4,512,64]{1,2,0:T(8,128)(2,1)S(1)} %copy.48), channel_id=1, replica_groups=mesh['fs'=4,'tp'=4,'rep'=2] {'fs'}, dimensions={0} | all-to-all | bytes 524288 | tf_op jit(solution)/shard_map/all_to_all | solution.py:51
  299.5 3.5 %all-to-all-start.4 = ((bf16[4,512,256]{2,1,0:T(8,128)(2,1)}), bf16[4,512,256]{2,1,0:T(8,128)(2,1)S(1)}, u32[]{:S(2)}, u32[]{:S(2)}) async-start(bf16[4,512,256]{2,1,0:T(8,128)(2,1)} %bitcast.11), calls=%async_computation.4 | async-start | bytes 2097152 | tf_op jit(solution)/shard_map/all_to_all | solution.py:51
  303.1 0.0 copy-done.6
  303.1 0.2 copy.49
  303.3 0.1 convert_multiply_fusion.2
  303.4 0.1 bitcast_subtract_fusion
  303.5 1.0 copy.50
  304.5 1.0 copy.51
  305.5 22.7 %all-to-all-done.4 = bf16[4,512,256]{2,1,0:T(8,128)(2,1)S(1)} async-done(((bf16[4,512,256]{2,1,0:T(8,128)(2,1)}), bf16[4,512,256]{2,1,0:T(8,128)(2,1)S(1)}, u32[]{:S(2)}, u32[]{:S(2)}) %all-to-all-start.4) | async-done | bytes 1048608 | tf_op jit(solution)/shard_map/all_to_all | solution.py:51
  328.1 0.4 fusion.1
  328.5 0.3 copy.54
  328.8 0.0 copy-start.3
  328.8 1.6 copy.55
  330.5 0.7 copy-done.3
  331.2 1.7 sub.6
Async XLA Ops:
  2.9 8.8 %all-to-all-start.2 = ((bf16[2,512,256]{2,1,0:T(8,128)(2,1)}), bf16[2,512,256]{2,1,0:T(8,128)(2,1)S(1)}, u32[]{:S(2)}, u32[]{:S(2)}) async-start(bf16[2,512,256]{2,1,0:T(8,128)(2,1)} %copy.42), calls=%async_computation.2 | async-start | bytes 1048576 | tf_op jit(solution)/shard_map/all_to_all | solution.py:35
  11.6 4.0 %copy-start.5 = (f32[512,256]{1,0:T(8,128)S(1)}, f32[512,256]{1,0:T(8,128)}, u32[]{:S(2)}) copy-start(f32[512,256]{1,0:T(8,128)} %param.10) | copy-start | bytes 1572868
  11.6 6.8 %all-to-all-start = ((bf16[2,512,1024]{2,1,0:T(8,128)(2,1)}), bf16[2,512,1024]{2,1,0:T(8,128)(2,1)S(1)}, u32[]{:S(2)}, u32[]{:S(2)}) async-start(bf16[2,512,1024]{2,1,0:T(8,128)(2,1)} %copy.39), calls=%async_computation | async-start | bytes 4194304 | tf_op jit(solution)/shard_map/all_to_all | solution.py:35
  18.4 15.6 %all-to-all-start.3 = ((bf16[4,512,64]{1,2,0:T(8,128)(2,1)}), bf16[4,512,64]{1,2,0:T(8,128)(2,1)S(1)}, u32[]{:S(2)}, u32[]{:S(2)}) async-start(bf16[4,512,64]{1,2,0:T(8,128)(2,1)} %bitcast.7), calls=%async_computation.3 | async-start | bytes 524288 | tf_op jit(solution)/shard_map/all_to_all | solution.py:43
  24.8 1.6 copy-start.2
  34.0 27.7 %all-to-all-start.1 = ((bf16[4,512,256]{2,1,0:T(8,128)(2,1)}), bf16[4,512,256]{2,1,0:T(8,128)(2,1)S(1)}, u32[]{:S(2)}, u32[]{:S(2)}) async-start(bf16[4,512,256]{2,1,0:T(8,128)(2,1)} %bitcast.38), calls=%async_computation.1 | async-start | bytes 2097152 | tf_op jit(solution)/shard_map/all_to_all | solution.py:43
  62.1 2.7 collective-permute-start
  65.0 5.1 %copy-start.1 = (bf16[2048,512]{1,0:T(8,128)(2,1)}, bf16[2048,512]{1,0:T(8,128)(2,1)S(1)}, u32[]{:S(2)}) copy-start(bf16[2048,512]{1,0:T(8,128)(2,1)S(1)} %pad_maximum_fusion.x_ref.v_ref) | copy-start | bytes 6291460
  174.3 2.1 copy-start
  282.1 4.2 %copy-start.4 = (bf16[2048,512]{1,0:T(8,128)(2,1)S(1)}, bf16[2048,512]{1,0:T(8,128)(2,1)}, u32[]{:S(2)}) copy-start(bf16[2048,512]{1,0:T(8,128)(2,1)} %chain.1) | copy-start | bytes 6291460
  283.6 2.7 collective-permute-start.1
  287.5 15.6 %copy-start.6 = (f32[512,256]{1,0:T(8,128)S(1)}, f32[512,256]{1,0:T(8,128)}, u32[]{:S(2)}) copy-start(f32[512,256]{1,0:T(8,128)} %param.9) | copy-start | bytes 1572868
  299.5 28.6 %all-to-all-start.4 = ((bf16[4,512,256]{2,1,0:T(8,128)(2,1)}), bf16[4,512,256]{2,1,0:T(8,128)(2,1)S(1)}, u32[]{:S(2)}, u32[]{:S(2)}) async-start(bf16[4,512,256]{2,1,0:T(8,128)(2,1)} %bitcast.11), calls=%async_computation.4 | async-start | bytes 2097152 | tf_op jit(solution)/shard_map/all_to_all | solution.py:51
  328.8 2.4 copy-start.3

commit v2 on v1

--- a/solution.py
+++ b/solution.py
@@ -77,24 +77,138 @@
                 ]
 
 
+def grams_kernel(xu, xo, o_ref, v_ref, whole, sem):
+    t, r = lax.axis_index("tp"), lax.axis_index("rep")
+    width = v_ref.shape[1]
+
+    @pl.when(r == 0)
+    def _():
+        gram_kernel(xu, o_ref)
+        v_ref[...] = xu[...]
+
+    @pl.when(r == 1)
+    def _():
+        load = pltpu.make_async_copy(xo, whole, sem)
+        load.start()
+        load.wait()
+        gram_kernel(whole, o_ref)
+        v_ref[...] = whole[:, pl.ds(pl.multiple_of(t * width, width), width)]
+
+
+def packed_shape(size):
+    return jax.ShapeDtypeStruct((len(blocks_of(CUTS)) * (size // CUTS), size // CUTS), BF)
+
+
 def gram(x):
     size, width = x.shape
-    step = size // CUTS
-    count = len(blocks_of(CUTS))
+    packed = packed_shape(size)
     return pl.pallas_call(
         gram_kernel,
         name="gram",
-        out_shape=jax.ShapeDtypeStruct((count * step, step), BF),
+        out_shape=packed,
         in_specs=[pl.BlockSpec(memory_space=pltpu.VMEM)],
         out_specs=pl.BlockSpec(memory_space=pltpu.VMEM),
         compiler_params=pltpu.CompilerParams(vmem_limit_bytes=48 << 20),
         cost_estimate=pl.CostEstimate(
-            flops=2 * width * count * step * step, bytes_accessed=2 * size * width, transcendentals=0
+            flops=2 * width * math.prod(packed.shape), bytes_accessed=2 * size * width, transcendentals=0
         ),
     )(x)
 
 
+def grams(xu, xo):
+    size, width = xu.shape
+    packed = packed_shape(size)
+    vmem = pl.BlockSpec(memory_space=pltpu.VMEM)
+    return pl.pallas_call(
+        grams_kernel,
+        name="grams",
+        out_shape=[packed, jax.ShapeDtypeStruct(xu.shape, BF)],
+        in_specs=[vmem, pl.BlockSpec(memory_space=pl.ANY)],
+        out_specs=[vmem, vmem],
+        scratch_shapes=[pltpu.VMEM(xo.shape, BF), pltpu.SemaphoreType.DMA],
+        compiler_params=pltpu.CompilerParams(vmem_limit_bytes=48 << 20),
+        cost_estimate=pl.CostEstimate(
+            flops=2 * size * math.prod(packed.shape), bytes_accessed=2 * size * size, transcendentals=0
+        ),
+    )(xu, xo)
+
+
+MESH = pl.DeviceIdType.MESH
+
+
+def greet(peers):
+    barrier = pltpu.get_barrier_semaphore()
+    for peer in peers:
+        pl.semaphore_signal(barrier, inc=1, device_id=peer, device_id_type=MESH)
+    pl.semaphore_wait(barrier, len(peers))
+
+
+class Copies:
+    def __init__(self, send, recv, anyone):
+        self.send, self.recv, self.anyone, self.started = send, recv, anyone, []
+
+    def make(self, key, src, dst, peer):
+        return pltpu.make_async_remote_copy(
+            src_ref=src,
+            dst_ref=dst,
+            send_sem=self.send.at[key],
+            recv_sem=self.recv.at[key],
+            device_id=peer,
+            device_id_type=MESH,
+        )
+
+    def start(self, key, src, dst, peer):
+        copy = self.make(key, src, dst, peer)
+        copy.start()
+        self.started.append(copy)
+
+    def arrived(self, key, dst):
+        self.make(key, dst, dst, self.anyone).wait_recv()
+
+    def sent(self):
+        for copy in self.started:
+            copy.wait_send()
+        self.started = []
+
+
 S1X, S1Y, S2X0, S2X1, S2Y0, S2Y1, RZ, AZ, AX, AY, AD0, AD1 = range(12)
+
+
+class Spread:
+    def __init__(self, copies, at, planes, z, t, r):
+        self.copies, self.at, self.planes = copies, at, planes
+        self.z, self.t, self.r = z, t, r
+        self.to_x, self.to_y = (z, t ^ 1, r), (z, t ^ 2, r)
+
+    def to_neighbours(self, m):
+        place = self.at(m, self.t, None)
+        self.copies.start((AX, m), place, place, self.to_x)
+        self.copies.start((AY, m), place, place, self.to_y)
+
+    def to_corner(self, m):
+        self.copies.arrived((AX, m), self.at(m, self.t ^ 1, None))
+        place = self.at(m, self.t ^ 1, 0)
+        self.copies.start((AD0, m), place, place, self.to_y)
+        self.copies.arrived((AY, m), self.at(m, self.t ^ 2, None))
+        place = self.at(m, self.t ^ 2, 1)
+        self.copies.start((AD1, m), place, place, self.to_x)
+
+    def along(self):
+        place = self.at(0, self.t, None)
+        for m in range(1, self.planes):
+            self.copies.start((AZ, m), place, place, (self.z ^ m, self.t, self.r))
+
+    def rest(self):
+        before = 0
+        for m in range(1, self.planes):
+            self.copies.arrived((AZ, m), self.at(m, self.t, None))
+            self.to_neighbours(m)
+            self.to_corner(before)
+            before = m
+        self.to_corner(before)
+        for m in range(self.planes):
+            self.copies.arrived((AD0, m), self.at(m, self.t ^ 3, 0))
+            self.copies.arrived((AD1, m), self.at(m, self.t ^ 3, 1))
 
 
 def reduce_kernel(planes, g_ref, o_ref, first, second, mixed, third, moved, own, send, recv):
@@ -105,102 +219,70 @@
     to_x, to_y = (z, beside, r), (z, above, r)
     others = list(range(1, planes))
     order = others + [0]
-
-    barrier = pltpu.get_barrier_semaphore()
-    peers = [to_x, to_y] + [(z ^ m, t, r) for m in others]
-    for peer in peers:
-        pl.semaphore_signal(barrier, inc=1, device_id=peer, device_id_type=pl.DeviceIdType.MESH)
-    pl.semaphore_wait(barrier, len(peers))
+    greet([to_x, to_y] + [(z ^ m, t, r) for m in others])
 
     def chunk(m, s):
         return (z ^ m) * 4 + s
 
-    started = []
-
-    def copy(kind, m, src, dst, peer, start=True):
-        c = pltpu.make_async_remote_copy(
-            src_ref=src,
-            dst_ref=dst,
-            send_sem=send.at[kind, m],
-            recv_sem=recv.at[kind, m],
-            device_id=peer,
-            device_id_type=pl.DeviceIdType.MESH,
-        )
-        if start:
-            c.start()
-            started.append(c)
-        return c
-
-    def arrived(kind, m, dst):
-        copy(kind, m, dst, dst, to_x, start=False).wait_recv()
-
-    def corner_halves(m):
-        copy(S1Y, m, g_ref.at[chunk(m, corner), parts[0]], first.at[m, 0], to_y)
-        copy(S1X, m, g_ref.at[chunk(m, corner), parts[1]], first.at[m, 1], to_x)
-
-    def direct_halves(m):
-        copy(S2X1, m, g_ref.at[chunk(m, beside), parts[1]], second.at[m, 0, parts[1]], to_x)
-        copy(S2Y0, m, g_ref.at[chunk(m, above), parts[0]], second.at[m, 1, parts[0]], to_y)
-
-    corner_halves(order[0])
-    corner_halves(order[1])
-    direct_halves(order[0])
-    for k in range(planes + 1):
-        if k < planes:
-            m = order[k]
-            arrived(S1Y, m, first.at[m, 0])
-            mixed[m, 0] = (g_ref[chunk(m, beside), parts[0]].astype(F32) + first[m, 0].astype(F32)).astype(BF)
-            copy(S2X0, m, mixed.at[m, 0], second.at[m, 0, parts[0]], to_x)
-            arrived(S1X, m, first.at[m, 1])
-            mixed[m, 1] = (g_ref[chunk(m, above), parts[1]].astype(F32) + first[m, 1].astype(F32)).astype(BF)
-            copy(S2Y1, m, mixed.at[m, 1], second.at[m, 1, parts[1]], to_y)
-            if k + 2 < planes:
-                corner_halves(order[k + 2])
-            if k + 1 < planes:
-                direct_halves(order[k + 1])
-        if k >= 1:
-            m = order[k - 1]
-            arrived(S2X1, m, second.at[m, 0, parts[1]])
-            arrived(S2Y0, m, second.at[m, 1, parts[0]])
-            arrived(S2X0, m, second.at[m, 0, parts[0]])
-            arrived(S2Y1, m, second.at[m, 1, parts[1]])
-            value = g_ref[chunk(m, t)].astype(F32) + second[m, 0].astype(F32) + second[m, 1].astype(F32)
-            if m:
-                moved[m] = value.astype(BF)
-                copy(RZ, m, moved.at[m], third.at[m], (z ^ m, t, r))
-            else:
-                own[...] = value
-    value = own[...]
-    for m in others:
-        arrived(RZ, m, third.at[m])
-        value = value + third[m].astype(F32)
-    o_ref[chunk(0, t)] = value.astype(BF)
-
-    def to_neighbours(m):
-        copy(AX, m, o_ref.at[chunk(m, t)], o_ref.at[chunk(m, t)], to_x)
-        copy(AY, m, o_ref.at[chunk(m, t)], o_ref.at[chunk(m, t)], to_y)
-
-    def to_corner(m):
-        arrived(AX, m, o_ref.at[chunk(m, beside)])
-        copy(AD0, m, o_ref.at[chunk(m, beside), parts[0]], o_ref.at[chunk(m, beside), parts[0]], to_y)
-        arrived(AY, m, o_ref.at[chunk(m, above)])
-        copy(AD1, m, o_ref.at[chunk(m, above), parts[1]], o_ref.at[chunk(m, above), parts[1]], to_x)
-
-    to_neighbours(0)
-    for m in others:
-        copy(AZ, m, o_ref.at[chunk(0, t)], o_ref.at[chunk(0, t)], (z ^ m, t, r))
-    before = 0
-    for m in others:
-        arrived(AZ, m, o_ref.at[chunk(m, t)])
-        to_neighbours(m)
-        to_corner(before)
-        before = m
-    to_corner(before)
-    for m in [0] + others:
-        arrived(AD0, m, o_ref.at[chunk(m, corner), parts[0]])
-        arrived(AD1, m, o_ref.at[chunk(m, corner), parts[1]])
-    for c in started:
-        c.wait_send()
+    @pl.when(r == 1)
+    def _():
+        o_ref[...] = g_ref[...]
+
+    @pl.when(r == 0)
+    def _():
+        copies = Copies(send, recv, to_x)
+
+        def corner_halves(m):
+            copies.start((S1Y, m), g_ref.at[chunk(m, corner), parts[0]], first.at[m, 0], to_y)
+            copies.start((S1X, m), g_ref.at[chunk(m, corner), parts[1]], first.at[m, 1], to_x)
+
+        def direct_halves(m):
+            copies.start((S2X1, m), g_ref.at[chunk(m, beside), parts[1]], second.at[m, 0, parts[1]], to_x)
+            copies.start((S2Y0, m), g_ref.at[chunk(m, above), parts[0]], second.at[m, 1, parts[0]], to_y)
+
+        corner_halves(order[0])
+        corner_halves(order[1])
+        direct_halves(order[0])
+        for k in range(planes + 1):
+            if k < planes:
+                m = order[k]
+                copies.arrived((S1Y, m), first.at[m, 0])
+                mixed[m, 0] = (g_ref[chunk(m, beside), parts[0]].astype(F32) + first[m, 0].astype(F32)).astype(BF)
+                copies.start((S2X0, m), mixed.at[m, 0], second.at[m, 0, parts[0]], to_x)
+                copies.arrived((S1X, m), first.at[m, 1])
+                mixed[m, 1] = (g_ref[chunk(m, above), parts[1]].astype(F32) + first[m, 1].astype(F32)).astype(BF)
+                copies.start((S2Y1, m), mixed.at[m, 1], second.at[m, 1, parts[1]], to_y)
+                if k + 2 < planes:
+                    corner_halves(order[k + 2])
+                if k + 1 < planes:
+                    direct_halves(order[k + 1])
+            if k >= 1:
+                m = order[k - 1]
+                copies.arrived((S2X1, m), second.at[m, 0, parts[1]])
+                copies.arrived((S2Y0, m), second.at[m, 1, parts[0]])
+                copies.arrived((S2X0, m), second.at[m, 0, parts[0]])
+                copies.arrived((S2Y1, m), second.at[m, 1, parts[1]])
+                value = g_ref[chunk(m, t)].astype(F32) + second[m, 0].astype(F32) + second[m, 1].astype(F32)
+                if m:
+                    moved[m] = value.astype(BF)
+                    copies.start((RZ, m), moved.at[m], third.at[m], (z ^ m, t, r))
+                else:
+                    own[...] = value
+        value = own[...]
+        for m in others:
+            copies.arrived((RZ, m), third.at[m])
+            value = value + third[m].astype(F32)
+        o_ref[chunk(0, t)] = value.astype(BF)
+
+        def at(m, s, which):
+            place = o_ref.at[chunk(m, s)]
+            return place if which is None else place.at[parts[which]]
+
+        spread = Spread(copies, at, planes, z, t, r)
+        spread.to_neighbours(0)
+        spread.along()
+        spread.rest()
+        copies.sent()
 
 
 def reduced(packed):
@@ -231,10 +313,224 @@
     return out.reshape(rows, width)
 
 
-def total_gram(packed):
+def front_kernel(
+    planes, um, ug, om, og, up_moment, out_moment, xu, xo, gu, go, mine, block, send, recv, pair_send, pair_recv,
+    up_send, up_recv, local,
+):
+    z, t, r = lax.axis_index("fs"), lax.axis_index("tp"), lax.axis_index("rep")
+    rows, cols = um.shape
+    narrow = om.shape[1]
+    step = cols // planes
+    partner = (z, t, 1 - r)
+    others = list(range(1, planes))
+    greet(
+        [partner, (z, t ^ 1, r), (z, t ^ 2, r)]
+        + [(z ^ m, t, c) for m in others for c in range(2)]
+    )
+    order = others[::-1] + [0]
+
+    def span(start, size):
+        return pl.ds(pl.multiple_of(start, size), size)
+
+    pairs = Copies(pair_send, pair_recv, partner)
+    for m in order:
+        pairs.start((m,), ug.at[:, span((1 - r) * cols + (z ^ m) * step, step)], gu.at[m], partner)
+    pairs.start((planes,), og.at[:, span((1 - r) * narrow, narrow)], go, partner)
+
+    ups = Copies(up_send, up_recv, partner)
+    target = xu.at[span(z * rows, rows), span(r * step, step)]
+    for m in order:
+        pairs.arrived((m,), gu.at[m])
+        place = span((z ^ m) * step, step)
+        grad = ug[:, span(r * cols + (z ^ m) * step, step)].astype(F32) + gu[m].astype(F32)
+        value = MOMENT * um[:, place] + grad
+        up_moment[:, place] = value
+        mine[m] = value.astype(BF)
+        if m:
+            for c in range(2):
+                @pl.when(r == c)
+                def _(m=m, c=c):
+                    ups.make((m, c), mine.at[m], target, (z ^ m, t, 0)).start()
+        else:
+            @pl.when(r == 1)
+            def _(m=m):
+                ups.make((0, 1), mine.at[m], target, (z, t, 0)).start()
+
+            @pl.when(r == 0)
+            def _(m=m):
+                xu[span(z * rows, rows), span(0, step)] = mine[m]
+
+    pairs.arrived((planes,), go)
+    grad = og[:, span(r * narrow, narrow)].astype(F32) + go[...].astype(F32)
+    value = MOMENT * om[...] + grad
+    out_moment[...] = value
+    block[...] = value.astype(BF)
+
+    def at(m, s, which):
+        first = s * 2 * narrow
+        if which is None:
+            return xo.at[span((z ^ m) * rows, rows), span(first, 2 * narrow)]
+        return xo.at[span((z ^ m) * rows, rows), span(first + which * narrow, narrow)]
+
+    def up_sent(c):
+        for m in order:
+            if m or c:
+                ups.make((m, c), mine.at[m], target, partner).wait_send()
+
+    @pl.when(r == 0)
+    def _():
+        copies = Copies(pair_send, pair_recv, partner)
+        copies.start((planes + 1,), block, at(0, t, 0), partner)
+        for m in order:
+            for c in range(2):
+                if m or c:
+                    place = xu.at[span((z ^ m) * rows, rows), span(c * step, step)]
+                    ups.arrived((m, c), place)
+        up_sent(0)
+        copies.sent()
+
+    @pl.when(r == 1)
+    def _():
+        keep = pltpu.make_async_copy(block, at(0, t, 1), local)
+        keep.start()
+        keep.wait()
+        pairs.arrived((planes + 1,), at(0, t, 0))
+        copies = Copies(send, recv, partner)
+        spread = Spread(copies, at, planes, z, t, r)
+        spread.to_neighbours(0)
+        up_sent(1)
+        spread.along()
+        spread.rest()
+        copies.sent()
+
+    pairs.sent()
+
+
+def front(um, ug, om, og):
+    planes = lax.axis_size("fs")
+    rows, cols = um.shape
+    narrow = om.shape[1]
+    step = cols // planes
+    vmem = pl.BlockSpec(memory_space=pltpu.VMEM)
+    return pl.pallas_call(
+        functools.partial(front_kernel, planes),
+        name="front",
+        out_shape=[
+            jax.ShapeDtypeStruct(um.shape, F32),
+            jax.ShapeDtypeStruct(om.shape, F32),
+            jax.ShapeDtypeStruct((planes * rows, 2 * step), BF),
+            jax.ShapeDtypeStruct((planes * rows, 8 * narrow), BF),
+        ],
+        in_specs=[vmem] * 4,
+        out_specs=[vmem] * 3 + [pl.BlockSpec(memory_space=pl.ANY)],
+        scratch_shapes=[
+            pltpu.VMEM((planes, rows, step), BF),
+            pltpu.VMEM((rows, narrow), BF),
+            pltpu.VMEM((planes, rows, step), BF),
+            pltpu.VMEM((rows, narrow), BF),
+            pltpu.SemaphoreType.DMA((12, planes)),
+            pltpu.SemaphoreType.DMA((12, planes)),
+            pltpu.SemaphoreType.DMA((planes + 2,)),
+            pltpu.SemaphoreType.DMA((planes + 2,)),
+            pltpu.SemaphoreType.DMA((planes, 2)),
+            pltpu.SemaphoreType.DMA((planes, 2)),
+            pltpu.SemaphoreType.DMA,
+        ],
+        compiler_params=pltpu.CompilerParams(
+            collective_id=2, has_side_effects=True, vmem_limit_bytes=56 << 20
+        ),
+    )(um, ug, om, og)
+
+
+def back_kernel(planes, v_ref, ub, ob, up_send, up_recv, out_send, out_recv):
+    z, t, r = lax.axis_index("fs"), lax.axis_index("tp"), lax.axis_index("rep")
+    rows, cols = ub.shape
+    step = cols // planes
+    narrow = ob.shape[1]
+    partner = (z, t, 1 - r)
+    others = list(range(1, planes))
+    greet([partner] + [(z ^ m, t, c) for m in others for c in range(2)])
+
+    def span(start, size):
+        return pl.ds(pl.multiple_of(start, size), size)
+
+    ups = Copies(up_send, up_recv, partner)
+    outs = Copies(out_send, out_recv, partner)
+    target = ub.at[:, span(z * step, step)]
+
+    def piece(m, c):
+        return v_ref.at[span((z ^ m) * rows, rows), pl.ds(c * step, step)]
+
+    @pl.when(r == 0)
+    def _():
+        for m in others[::-1] + [0]:
+            for c in range(2):
+                if m or c:
+                    pltpu.make_async_remote_copy(
+                        src_ref=piece(m, c), dst_ref=target, send_sem=up_send.at[m, c], recv_sem=up_recv.at[m, 0],
+                        device_id=(z ^ m, t, c), device_id_type=MESH,
+                    ).start()
+        ub[:, span(z * step, step)] = v_ref[span(z * rows, rows), pl.ds(0, step)]
+        outs.arrived((0,), ob)
+
+    @pl.when(r == 1)
+    def _():
+        outs.start((0,), v_ref.at[span(z * rows, rows), pl.ds(0, narrow)], ob, partner)
+        ob[...] = v_ref[span(z * rows, rows), pl.ds(narrow, narrow)]
+        ups.arrived((0, 0), target)
+        outs.sent()
+
+    for m in others:
+        ups.arrived((m, 0), ub.at[:, span((z ^ m) * step, step)])
+
+    @pl.when(r == 0)
+    def _():
+        for m in others[::-1] + [0]:
+            for c in range(2):
+                if m or c:
+                    ups.make((m, c), piece(m, c), target, partner).wait_send()
+
+
+def back(v, rows, cols, narrow):
+    planes = lax.axis_size("fs")
+    vmem = pl.BlockSpec(memory_space=pltpu.VMEM)
+    return pl.pallas_call(
+        functools.partial(back_kernel, planes),
+        name="back",
+        out_shape=[jax.ShapeDtypeStruct((rows, cols), BF), jax.ShapeDtypeStruct((rows, narrow), BF)],
+        in_specs=[vmem],
+        out_specs=[vmem] * 2,
+        scratch_shapes=[
+            pltpu.SemaphoreType.DMA((planes, 2)),
+            pltpu.SemaphoreType.DMA((planes, 2)),
+            pltpu.SemaphoreType.DMA((1,)),
+            pltpu.SemaphoreType.DMA((1,)),
+        ],
+        compiler_params=pltpu.CompilerParams(
+            collective_id=3, has_side_effects=True, vmem_limit_bytes=32 << 20
+        ),
+    )(v)
+
+
+def square_of_four(um, om):
     fs, tp, rep = (lax.axis_size(name) for name in ("fs", "tp", "rep"))
-    if rep == 2 and tp == 4 and fs & (fs - 1) == 0 and packed.shape[0] % (fs * tp * 32) == 0:
-        return reduced(packed)
+    step, blocks = um.shape[1] // fs, len(blocks_of(CUTS))
+    size = um.shape[0] * fs
+    return (
+        rep == 2
+        and tp == 4
+        and fs > 1
+        and fs & (fs - 1) == 0
+        and um.shape[0] % 16 == 0
+        and step % 128 == 0
+        and om.shape[1] == step
+        and size == 8 * om.shape[1]
+        and blocks * (size // CUTS) % (fs * tp * 32) == 0
+    )
+
+
+def summed(packed):
+    rep = lax.axis_size("rep")
     packed = lax.psum(packed, ("fs", "tp"))
     if rep > 2:
         groups = [[i for i in range(rep) if i % 2 == k] for k in range(2)]
@@ -333,23 +629,37 @@
     )(packed, v)
 
 
-def on_device(up_weight, up_momentum, up_grads, out_weight, out_momentum, out_grads):
+def by_kernels(up_momentum, up_grads, out_momentum, out_grads):
+    up_moment, out_moment, xu, xo = front(up_momentum, up_grads, out_momentum, out_grads)
+    packed, values = grams(xu, xo)
+    final = chain(reduced(packed), values)
+    up, out = back(final, *up_momentum.shape, out_momentum.shape[1])
+    return up_moment, out_moment, up, out
+
+
+def by_collectives(up_momentum, up_grads, out_momentum, out_grads):
     even = lax.axis_index("rep") % 2 == 0
-    up_moment = MOMENT * up_momentum + reduced_grad(up_grads[0])
-    out_moment = MOMENT * out_momentum + reduced_grad(out_grads[0])
+    up_moment = MOMENT * up_momentum + reduced_grad(up_grads)
+    out_moment = MOMENT * out_momentum + reduced_grad(out_grads)
     up = to_columns(up_moment.astype(BF))
     out = to_columns(out_moment.astype(BF))
     width, narrow = up.shape[1], out.shape[1]
     out = jnp.pad(out, ((0, 0), (0, width - narrow)))
     other = swap_pairs(jnp.where(even, out, up))
     values = jnp.concatenate([jnp.where(even, up, out), other], axis=1)
-    final = chain(total_gram(gram(values)), values)
+    final = chain(summed(gram(values)), values)
     mine, other = final[:, :width], swap_pairs(final[:, width:])
-    up = to_rows(jnp.where(even, mine, other)).astype(F32)
-    out = to_rows(jnp.where(even, other, mine)[:, :narrow]).astype(F32)
+    up = to_rows(jnp.where(even, mine, other))
+    out = to_rows(jnp.where(even, other, mine)[:, :narrow])
+    return up_moment, out_moment, up, out
+
+
+def on_device(up_weight, up_momentum, up_grads, out_weight, out_momentum, out_grads):
+    way = by_kernels if square_of_four(up_momentum, out_momentum) else by_collectives
+    up_moment, out_moment, up, out = way(up_momentum, up_grads[0], out_momentum, out_grads[0])
     group = lax.axis_size("tp") * lax.axis_size("rep")
-    up_direction = up * math.sqrt(up_weight.shape[1] * group)
-    out_direction = out * math.sqrt(out_weight.shape[1] * group)
+    up_direction = up.astype(F32) * math.sqrt(up_weight.shape[1] * group)
+    out_direction = out.astype(F32) * math.sqrt(out_weight.shape[1] * group)
     return (
         up_weight - RATE * up_direction,
         up_moment,

time: 334 us -> 261 us (0.78)
  waiting for transfers between devices: 57.7 us -> 0 us
  Pallas kernels: 215 us -> 246 us
  starting transfers between devices: 20.9 us -> 0 us
  blocking collectives: 11.8 us -> 0 us
  local copies, waits for them, and re-layouts: 19.4 us -> 8.81 us
  other arithmetic: 7.23 us -> 3.85 us
    pallas_call x1 -> x3, Pallas kernels: 5.04 us -> 69 us  [the longest x1 36.4 us: front(): pl.pallas_call(functools.partial(front_kernel, planes), name='front', out...]
    all_to_all x5 -> x0, waiting for transfers between devices: 52.4 us -> none  [the longest x2 28.7 us: to_columns(): lax.all_to_all(pieces, 'fs', split_axis=0, concat_axis=0, tiled=True)]
    pallas_call x1, Pallas kernels: 104 us -> 71.1 us  [reduced(): pl.pallas_call(functools.partial(reduce_kernel, planes), name='reduced',...]
    all_to_all x5 -> x0, starting transfers between devices: 20.8 us -> none  [the longest x2 9.86 us: to_columns(): lax.all_to_all(pieces, 'fs', split_axis=0, concat_axis=0, tiled=True)]
    all_to_all x1 -> x0, blocking collectives: 11.8 us -> none  [to_rows(): lax.all_to_all(pieces, 'fs', split_axis=0, concat_axis=0, tiled=True)]
    ppermute x2 -> x0, waiting for transfers between devices: 5.29 us -> none  [swap_pairs(): return lax.ppermute(values, 'rep', [(i, i ^ 1) for i in range(size)])]
    mul x1 -> x2, other arithmetic: 0.08 us -> 3.85 us  [the longest x1 2.78 us: on_device(): up_direction = up.astype(F32) * math.sqrt(up_weight.shape[1] * group)]
    transpose x2 -> x0, local copies, waits for them, and re-layouts: 3.38 us -> none  [reduced_grad(): pieces = grads.reshape(rows, size, cols // size).transpose(1, 0, 2)]
  transfers between devices with their start and end apart: 7 -> 0, of which waited for: 6 -> 0; matrix products, arithmetic and copies ran while one was open for 4% -> 0% of each run, Pallas kernels for 0% -> 0%
where the time goes in v2:
time: 261 us; the launch traced here: 259 us
  Pallas kernels  246 us (94%)
  local copies, waits for them, and re-layouts  8.81 us (3%)
  other arithmetic  3.85 us (1%)
    pallas_call x1, Pallas kernels, chain(): pl.pallas_call(chain_kernel, name='chain', out_shape=jax.ShapeDtypeStruct...  106 us
    pallas_call x1, Pallas kernels, reduced(): pl.pallas_call(functools.partial(reduce_kernel, planes), name='reduced',...  71.1 us
    pallas_call x1, Pallas kernels, front(): pl.pallas_call(functools.partial(front_kernel, planes), name='front', out...  36.4 us
    pallas_call x1, Pallas kernels, back(): pl.pallas_call(functools.partial(back_kernel, planes), name='back', out_s...  27.2 us
    unnamed x18, local copies, waits for them, and re-layouts  8.81 us
    pallas_call x1, Pallas kernels, grams(): pl.pallas_call(grams_kernel, name='grams', out_shape=[packed, jax.ShapeDt...  5.34 us

profile of v2, /device:TPU:0, one launch (start us, length us, event | category | flops | bytes accessed | tf_op | source)
XLA Modules:
  0.0 259.0 jit_solution(11195446706647073153)
XLA Ops:
  0.6 36.4 %front.1 = (f32[512,1024]{1,0:T(8,128)}, f32[512,256]{1,0:T(8,128)}, bf16[2048,512]{1,0:T(8,128)(2,1)}, bf16[2048,2048]{1,0:T(8,128)(2,1)}) custom-call(f32[512,1024]{1,0:T(8,128)} %um.1, bf16[512,2048]{1,0:T(8,128)(2,1)} %bitcast.6, f32[512,256]{1,0:T(8,128)} %om.1, bf16[512,512]{1,0:T(8,128)(2,1)} %bitcast.7), custom_call_target="tpu_custom_call" | custom-call | tf_op jit(solution)/shard_map/front/pallas_call | solution.py:415
  37.0 0.0 copy-start.2
  37.0 1.6 copy-done.2
  38.6 5.3 %grams.1 = (bf16[9216,256]{1,0:T(8,128)(2,1)}, bf16[2048,512]{1,0:T(8,128)(2,1)S(1)}) custom-call(bf16[2048,512]{1,0:T(8,128)(2,1)S(1)} %copy-done.2, bf16[2048,2048]{1,0:T(8,128)(2,1)} %get-tuple-element.15.xo), custom_call_target="tpu_custom_call" | custom-call | flops 9663676416 | bytes 8388608 | tf_op jit(solution)/shard_map/grams/pallas_call | solution.py:122
  44.0 0.0 copy-start.3
  44.0 1.3 copy-done.3
  45.3 71.1 %reduced.1 = bf16[16,576,256]{2,1,0:T(8,128)(2,1)S(1)} custom-call(bf16[16,576,256]{2,1,0:T(8,128)(2,1)} %bitcast.5), custom_call_target="tpu_custom_call" | custom-call | tf_op jit(solution)/shard_map/reduced/pallas_call | solution.py:293
  116.4 0.0 copy-start
  116.4 2.1 copy-done
  118.6 0.0 copy-start.6
  118.6 105.5 %chain.1.v_ref = bf16[2048,512]{1,0:T(8,128)(2,1)} custom-call(bf16[9216,256]{1,0:T(8,128)(2,1)} %bitcast.4, bf16[2048,512]{1,0:T(8,128)(2,1)} %copy-done.3), custom_call_target="tpu_custom_call" | custom-call | flops 81604378624 | bytes 12582912 | tf_op jit(solution)/shard_map/chain/pallas_call | solution.py:620
  224.1 0.0 copy-start.1
  224.1 1.6 copy-done.1
  225.7 0.0 copy-start.4
  225.7 27.2 %back.1 = (bf16[512,1024]{1,0:T(8,128)(2,1)S(1)}, bf16[512,256]{1,0:T(8,128)(2,1)S(1)}) custom-call(bf16[2048,512]{1,0:T(8,128)(2,1)S(1)} %copy-done.1), custom_call_target="tpu_custom_call" | custom-call | tf_op jit(solution)/shard_map/back/pallas_call | solution.py:497
  252.9 0.0 copy-done.6
  252.9 1.1 convert_multiply_fusion.2
  254.0 0.0 copy-done.4
  254.0 0.0 copy-start.5
  254.0 2.8 %convert_multiply_fusion = (f32[512,1024]{1,0:T(8,128)}, f32[512,1024]{1,0:T(8,128)}) fusion(bf16[512,1024]{1,0:T(8,128)(2,1)S(1)} %get-tuple-element.18, f32[512,1024]{1,0:T(8,128)S(1)} %copy-done.4), kind=kLoop, calls=%fused_computation | loop fusion | flops 2097152 | bytes 7340032 | tf_op jit(solution)/shard_map/mul | solution.py:661
  256.8 0.0 copy-done.5
  256.8 0.0 copy-start.7
  256.8 1.3 copy.14
  258.1 0.1 copy-done.7
  258.2 0.8 copy.15
Async XLA Ops:
  37.0 1.6 copy-start.2
  44.0 1.3 copy-start.3
  116.4 2.1 copy-start
  118.6 134.4 %copy-start.6 = (f32[512,256]{1,0:T(8,128)S(1)}, f32[512,256]{1,0:T(8,128)}, u32[]{:S(2)}) copy-start(f32[512,256]{1,0:T(8,128)} %param.9) | copy-start | bytes 1572868
  224.1 1.6 copy-start.1
  225.7 28.3 %copy-start.4 = (f32[512,1024]{1,0:T(8,128)S(1)}, f32[512,1024]{1,0:T(8,128)}, u32[]{:S(2)}) copy-start(f32[512,1024]{1,0:T(8,128)} %param.6) | copy-start | bytes 6291460
  254.0 2.8 %copy-start.5 = (f32[512,1024]{1,0:T(8,128)S(1)}, f32[512,1024]{1,0:T(8,128)}, u32[]{:S(2)}) copy-start(f32[512,1024]{1,0:T(8,128)} %get-tuple-element.33) | copy-start | bytes 6291460
  256.8 1.4 copy-start.7
